TPU v7x, 128 devices: a whole 4x4x4 slice. The times are simulated.
128 devices in a mesh: rep: 2 (over z_hi), fs: 32 (over z_lo, y, x), tp: 2 (over core).
Axes of the slice: x: 4, y: 4, z: 4 (z_hi: 2, z_lo: 2; z = z_hi * 2 + z_lo), core: 2. Of those that a mesh axis runs over, the one named last changes fastest.
Arguments:
- hidden_in: bfloat16 [40960, 2048], P(('rep', 'fs'), 'tp'), may hold values from -6 to 6
- mix_gain: float32 [2048], replicated, may hold values from 0.1 to 1.9
- w_value: bfloat16 [2048, 1024], P('fs', 'tp'), may hold values from -0.125 to 0.125
- w_gate: bfloat16 [2048, 1024], P('fs', 'tp'), may hold values from -0.125 to 0.125
- conv_taps: float32 [31, 1024], P(None, 'tp'), may hold values from -5 to 5
- conv_bias: float32 [1024], P('tp'), may hold values from -3 to 3
- chan_gain: float32 [1024], P('tp'), may hold values from 0.1 to 1.9
- chan_bias: float32 [1024], P('tp'), may hold values from -3 to 3
- w_back: bfloat16 [1024, 2048], P('tp', 'fs'), may hold values from -0.1875 to 0.1875
- feed_gain: float32 [2048], replicated, may hold values from 0.1 to 1.9
- w_up: bfloat16 [2048, 8192], P(None, ('fs', 'tp')), may hold values from -0.125 to 0.125
- w_down: bfloat16 [8192, 2048], P(('fs', 'tp')), may hold values from -0.0625 to 0.0625
Outputs:
- layer_out: bfloat16 [40960, 2048], P(('rep', 'fs'), 'tp')
All inputs are finite; a program needn't handle non-finite values.
Results may differ from a plain program's by a relative error of at most 0.015.
Values may be sent and summed in bfloat16 or wider, within the bound.
A program may use at most 128 MiB of HBM per device.

v0:
```python
import jax
import jax.numpy as jnp
from jax import lax
from jax.sharding import PartitionSpec as P

KW = 31
LEN = 128


def copy_for_each(array, axis):
    copies = jnp.broadcast_to(array, (lax.axis_size(axis), *array.shape))
    return lax.all_to_all(copies, axis, split_axis=0, concat_axis=0, tiled=True)


def in_order(parts, dim):
    lengths = list(parts.shape[1:])
    lengths[dim] *= parts.shape[0]
    return jnp.moveaxis(parts, 0, dim).reshape(lengths)


def gathered_copies(array, axis, dim):
    parts = copy_for_each(array, axis)
    return in_order(parts, dim)


def side_by_side(arrays, axis, dim, along):
    widths = [a.shape[along] for a in arrays]
    both = jnp.concatenate(arrays, axis=along)
    result = lax.all_gather(both, axis, axis=dim, tiled=True)
    return tuple(jnp.split(result, [sum(widths[:k]) for k in range(1, len(widths))], axis=along))


def in_blocks(array, dim, count):
    lengths = array.shape
    parts = array.reshape(*lengths[:dim], count, lengths[dim] // count, *lengths[dim + 1 :])
    return jnp.moveaxis(parts, dim, 0)


def summed_on_arrival(array, axis, dim):
    count = lax.axis_size(axis)
    parts = lax.all_to_all(in_blocks(array, dim, count), axis, 0, 0, tiled=True)
    return jnp.sum(parts.astype(jnp.float32), axis=0)


def rms_norm(stream, gain):
    values = stream.astype(jnp.float32)
    scaled = values * lax.rsqrt(jnp.mean(values * values, axis=-1, keepdims=True) + 1e-06)
    return (scaled * gain).astype(jnp.bfloat16)


def causal_filter(gated, conv_taps, conv_bias):
    channels = gated.shape[1]
    blocks = gated.reshape(gated.shape[0] // LEN, LEN, channels)
    padded = jnp.pad(blocks, ((0, 0), (KW - 1, 0), (0, 0)))
    result = jnp.zeros_like(blocks) + conv_bias
    for tap_index in range(KW):
        result = result + conv_taps[tap_index] * padded[:, tap_index : tap_index + LEN]
    return result.reshape(gated.shape)


def shards(
    hidden_in,
    mix_gain,
    w_value,
    w_gate,
    conv_taps,
    conv_bias,
    chan_gain,
    chan_bias,
    w_back,
    feed_gain,
    w_up,
    w_down,
):
    gathered = gathered_copies(hidden_in, "tp", 1)
    normed = rms_norm(gathered, mix_gain)
    local_channels = w_value.shape[1]
    whole_value, whole_gate = side_by_side((w_value, w_gate), "fs", 0, 1)
    value_proj = jnp.dot(normed, whole_value, preferred_element_type=jnp.float32)
    gate_proj = jnp.dot(normed, whole_gate, preferred_element_type=jnp.float32)
    gated = value_proj * jax.nn.sigmoid(gate_proj)
    filtered = causal_filter(gated, conv_taps, conv_bias)
    channel_total = local_channels * lax.axis_size("tp")
    first_sum, square_sum = lax.psum(
        (jnp.sum(filtered, axis=1), jnp.sum(filtered * filtered, axis=1)), "tp"
    )
    chan_mean = (first_sum / channel_total)[:, None]
    chan_var = (square_sum / channel_total)[:, None] - chan_mean * chan_mean
    centred = (filtered - chan_mean) * lax.rsqrt(chan_var + 1e-05) * chan_gain + chan_bias
    mixer_act = jax.nn.silu(centred).astype(jnp.bfloat16)
    whole_back = gathered_copies(w_back, "fs", 1)
    partial_value = jnp.dot(mixer_act, whole_back, preferred_element_type=jnp.float32)
    summed = summed_on_arrival(partial_value.astype(jnp.bfloat16), "tp", 1)
    second = (hidden_in.astype(jnp.float32) + summed).astype(jnp.bfloat16)
    gathered_feed = lax.all_gather(second, "tp", axis=1, tiled=True)
    normed_feed = rms_norm(gathered_feed, feed_gain)
    up_proj = jnp.dot(
        normed_feed,
        lax.all_gather(w_up, "fs", axis=1, tiled=True),
        preferred_element_type=jnp.float32,
    )
    hidden = jnp.square(jax.nn.relu(up_proj)).astype(jnp.bfloat16)
    feed_partial = jnp.dot(
        hidden, lax.all_gather(w_down, "fs", axis=0, tiled=True), preferred_element_type=jnp.float32
    )
    feed = summed_on_arrival(feed_partial.astype(jnp.bfloat16), "tp", 1)
    return (second.astype(jnp.float32) + feed).astype(jnp.bfloat16)


def solution(mesh):
    placed = (
        P(("rep", "fs"), "tp"),
        P(),
        P("fs", "tp"),
        P("fs", "tp"),
        P(None, "tp"),
        P("tp"),
        P("tp"),
        P("tp"),
        P("tp", "fs"),
        P(),
        P(None, ("fs", "tp")),
        P(("fs", "tp"), None),
    )
    return jax.shard_map(
        shards, mesh=mesh, in_specs=placed, out_specs=P(("rep", "fs"), "tp"), check_vma=False
    )
```

profile of v0, /device:TPU:1, one launch (start us, length us, event | category | flops | bytes accessed | tf_op | source)
XLA Modules:
  0.0 708.8 jit_solution(11881618682649393780)
XLA Ops:
  6.5 1.5 pad_maximum_fusion
  8.1 1.7 copy.15
  10.0 7.0 all_to_all.20
  17.0 1.6 broadcast_in_dim.5
  18.6 8.6 %all-to-all-start.1 = ((bf16[32,512,64]{1,2,0:T(8,128)(2,1)}), bf16[32,512,64]{1,2,0:T(8,128)(2,1)}, u32[]{:S(2)}, u32[]{:S(2)}) async-start(bf16[32,512,64]{1,2,0:T(8,128)(2,1)} %broadcast_in_dim.5), calls=%async_computation.1 | async-start | bytes 4194304 | tf_op jit(solution)/shard_map/all_to_all | solution.py:12
  27.3 0.6 multiply_reduce_fusion
  28.2 2.2 fusion.4
  30.4 127.4 %all-gather.5.cloned.1.call-done = bf16[2048,1024]{1,0:T(8,128)(2,1)} async-done(((bf16[64,1024]{1,0:T(8,128)(2,1)}), bf16[2048,1024]{1,0:T(8,128)(2,1)}) %all-gather.5.cloned.1.call-update) | async-done | bytes 4194320 | tf_op jit(solution)/shard_map/all_gather | solution.py:29
  157.8 4.2 fusion.28
  162.1 1.6 fusion.16
  163.7 5.5 fusion.93
  169.2 22.1 %all-reduce.1 = (f32[640]{0:T(1024)S(1)}, f32[640]{0:T(1024)S(1)}) all-reduce(f32[640]{0:T(1024)S(1)} %bitcast.77, f32[640]{0:T(1024)S(1)} %bitcast.76), channel_id=1, replica_groups=mesh['rep'=2,'fs'=32,'tp'=2] {'tp'}, use_global_device_ids=true, to_apply=%region_4.5 | all-reduce | flops 1280 | bytes 10240 | tf_op jit(solution)/shard_map/psum | solution.py:84
  191.2 0.5 multiply_convert_fusion.1
  191.8 3.1 convolution_convert_fusion
  194.9 0.3 copy.23
  195.2 5.8 all_to_all.21
  201.0 0.6 convert_reduce_fusion.1
  201.6 0.7 copy-done.2
  202.3 1.5 add_convert_fusion.1
  204.0 0.7 all-gather.11.cloned.1.call-update
  204.6 0.2 all-gather.9.cloned.1.call-start
  204.9 0.3 all-gather.9.cloned.1.call-update
  205.2 13.4 %all-gather.7.cloned.1.call-done = bf16[640,2048]{1,0:T(8,128)(2,1)} async-done(((bf16[640,1024]{1,0:T(8,128)(2,1)}), bf16[640,2048]{1,0:T(8,128)(2,1)}) %all-gather.7.cloned.1.call-update) | async-done | bytes 2621456 | tf_op jit(solution)/shard_map/all_gather | solution.py:95
  218.7 2.5 fusion
  221.2 190.3 %all-gather.11.cloned.1.call-done = bf16[4096,2048]{1,0:T(8,128)(2,1)} async-done(((bf16[128,2048]{1,0:T(8,128)(2,1)}), bf16[4096,2048]{1,0:T(8,128)(2,1)}) %all-gather.11.cloned.1.call-update) | async-done | bytes 16777232 | tf_op jit(solution)/shard_map/all_gather | solution.py:104
  411.5 222.9 %all-gather.9.cloned.1.call-done = bf16[2048,4096]{1,0:T(8,128)(2,1)} async-done(((bf16[2048,128]{1,0:T(8,128)(2,1)}), bf16[2048,4096]{1,0:T(8,128)(2,1)}) %all-gather.9.cloned.1.call-update) | async-done | bytes 16777232 | tf_op jit(solution)/shard_map/all_gather | solution.py:99
  634.4 33.8 %convolution_convert_fusion.1 = bf16[640,2048]{1,0:T(8,128)(2,1)} fusion(bf16[4096,2048]{1,0:T(8,128)(2,1)} %all-gather.11.cloned.1.call-done, bf16[2048,4096]{1,0:T(8,128)(2,1)} %all-gather.9.cloned.1.call-done, bf16[640,2048]{1,0:T(8,128)(2,1)S(1)} %copy-done.3, f32[2048]{0:T(1024)S(1)} %copy-done.11, f32[640]{0:T(1024)S(1)} %add_rsqrt_fusion), kind=kOutput, calls=%fused_computation.43 | convolution fusion | flops 21489254400 | bytes 38808064 | tf_op jit(solution)/shard_map/dot_general | solution.py:103
  668.2 2.0 copy.22
  670.2 29.3 %all_to_all.22 = bf16[2,640,1024]{2,1,0:T(8,128)(2,1)S(1)} all-to-all(bf16[2,640,1024]{2,1,0:T(8,128)(2,1)S(1)} %bitcast.71), channel_id=1, replica_groups=mesh['rep'=2,'fs'=32,'tp'=2] {'tp'}, dimensions={0} | all-to-all | bytes 5242880 | tf_op jit(solution)/shard_map/all_to_all | solution.py:41
  699.4 0.6 convert_reduce_fusion
  700.0 0.7 copy-done
  700.8 1.5 add_convert_fusion
  (34 shorter events, 0.6 us)
Async XLA Ops:
  6.5 151.2 %all-gather.5.cloned.1.call-start = ((), (), s32[]{:S(2)}) async-start(), calls=%async_computation.4 | async-start | bytes 4325376 | tf_op jit(solution)/shard_map/all_gather | solution.py:29
  10.0 7.0 copy-start.5
  18.6 173.2 %all-to-all-start.1 = ((bf16[32,512,64]{1,2,0:T(8,128)(2,1)}), bf16[32,512,64]{1,2,0:T(8,128)(2,1)}, u32[]{:S(2)}, u32[]{:S(2)}) async-start(bf16[32,512,64]{1,2,0:T(8,128)(2,1)} %broadcast_in_dim.5), calls=%async_computation.1 | async-start | bytes 4194304 | tf_op jit(solution)/shard_map/all_to_all | solution.py:12
  27.3 0.8 copy-start.6
  27.3 0.9 copy-start.7
  27.3 191.4 %all-gather.7.cloned.1.call-start = ((), (), s32[]{:S(2)}) async-start(), calls=%async_computation.5 | async-start | bytes 3932160 | tf_op jit(solution)/shard_map/all_gather | solution.py:95
  30.4 131.7 %copy-start.1 = (bf16[640,2048]{0,1:T(8,128)(2,1)S(1)}, bf16[640,2048]{0,1:T(8,128)(2,1)}, u32[]{:S(2)}) copy-start(bf16[640,2048]{0,1:T(8,128)(2,1)} %fusion.4) | copy-start | bytes 7864324
  157.8 4.3 copy-start.4
  162.0 1.6 copy-start.8
  163.7 27.6 %copy-start.9 = (f32[512]{0:T(512)S(1)}, f32[512]{0:T(512)}, u32[]{:S(2)}) copy-start(f32[512]{0:T(512)} %param.19) | copy-start | bytes 6148
  163.7 27.6 %copy-start.10 = (f32[512]{0:T(512)S(1)}, f32[512]{0:T(512)}, u32[]{:S(2)}) copy-start(f32[512]{0:T(512)} %param.18) | copy-start | bytes 6148
  201.0 1.3 copy-start.2
  203.9 207.6 %all-gather.11.cloned.1.call-start = ((), (), s32[]{:S(2)}) async-start(), calls=%async_computation.7 | async-start | bytes 17301504 | tf_op jit(solution)/shard_map/all_gather | solution.py:104
  204.6 429.8 %all-gather.9.cloned.1.call-start = ((), (), s32[]{:S(2)}) async-start(), calls=%async_computation.6 | async-start | bytes 17301504 | tf_op jit(solution)/shard_map/all_gather | solution.py:99
  205.2 429.2 %copy-start.11 = (f32[2048]{0:T(1024)S(1)}, f32[2048]{0:T(1024)}, u32[]{:S(2)}) copy-start(f32[2048]{0:T(1024)} %param.21) | copy-start | bytes 24580
  218.7 415.7 %copy-start.3 = (bf16[640,2048]{1,0:T(8,128)(2,1)S(1)}, bf16[640,2048]{1,0:T(8,128)(2,1)}, u32[]{:S(2)}) copy-start(bf16[640,2048]{1,0:T(8,128)(2,1)} %all-gather.7.cloned.1.call-done) | copy-start | bytes 7864324
  699.4 1.3 copy-start
Sparse Core Ops, SparseCore 0:
  9.0 148.7 all-gather.4
  204.0 14.6 all-gather.6
  220.3 191.0 all-gather.10
  412.9 221.4 all-gather.8
where the time goes:
time: 709 us
  waiting for transfers between devices  555 us (78%)
  blocking collectives  64.1 us (9%)
  matrix products  42.7 us (6%)
  other arithmetic  17 us (2%)
  between operations  13.3 us (2%)
  starting transfers between devices  8.94 us (1%)
  local copies, waits for them, and re-layouts  7.52 us (1%)
    all_gather x1, waiting for transfers between devices, shards(): lax.all_gather(w_up, 'fs', axis=1, tiled=True)  223 us
    all_gather x1, waiting for transfers between devices, shards(): lax.all_gather(w_down, 'fs', axis=0, tiled=True)  190 us
    all_gather x1, waiting for transfers between devices, side_by_side(): result = lax.all_gather(both, axis, axis=dim, tiled=True)  127 us
    all_to_all x2, blocking collectives, summed_on_arrival(): parts = lax.all_to_all(in_blocks(array, dim, count), axis, 0, 0, tiled=True)  35.1 us
    dot_general x1, matrix products, shards(): jnp.dot(hidden, lax.all_gather(w_down, 'fs', axis=0, tiled=True), preferr...  33.8 us
    psum x1, blocking collectives, shards(): lax.psum((jnp.sum(filtered, axis=1), jnp.sum(filtered * filtered, axis=1)...  22.1 us
  transfers between devices with their start and end apart: 5, of which 4 were waited for; matrix products, arithmetic and copies ran while one was open for 3% of the time, Pallas kernels for 0%

commit v1 on v0

v1 whole, which is shorter than its diff:
```python
import functools

import jax
import jax.numpy as jnp
from jax import lax
from jax.experimental import pallas as pl
from jax.experimental.pallas import tpu as pltpu
from jax.sharding import PartitionSpec as P

KW = 31
LEN = 128
SIDE = 4
F32 = jnp.float32
BF16 = jnp.bfloat16
UP_PIECES = 4
DOWN_PIECES = 4
PIECES = 2 + UP_PIECES + DOWN_PIECES


def kernel(
    x_hbm, mix_gain, wv_hbm, wg_hbm, taps, conv_bias, chan_gain, chan_bias, wb_hbm, feed_gain, wu_hbm, wd_hbm,
    out_hbm,
    conv_w, up_w, down_w, x_full, normed, padded, filtered, act, stat_own, stat_got,
    mix_send, mix_got, second, hidden, part_send, part_got, keep, own_sum, ret_send, ret_got, out_vmem,
    load_sem, send_sem, recv_sem, z_send, z_recv, pair_send, pair_recv, hop_send, hop_recv, out_sem,
):
    rows, half = x_hbm.shape
    features = 2 * half
    channels = wv_hbm.shape[1]
    k_rows = wv_hbm.shape[0]
    block = wu_hbm.shape[1]
    sequences = rows // LEN
    part_rows = rows // 2

    core = lax.axis_index("tp")
    other = 1 - core
    place = lax.axis_index("fs")
    z_hi = lax.axis_index("rep")
    x = lax.rem(place, SIDE)
    y = lax.rem(place // SIDE, SIDE)
    z_lo = place // (SIDE * SIDE)
    z = z_hi * 2 + z_lo
    x_next, x_prev = lax.rem(x + 1, SIDE), lax.rem(x + SIDE - 1, SIDE)
    y_next, y_prev = lax.rem(y + 1, SIDE), lax.rem(y + SIDE - 1, SIDE)
    z_next, z_prev = lax.rem(z + 1, 4), lax.rem(z + 3, 4)

    def at_x(xx):
        return {"fs": z_lo * SIDE * SIDE + y * SIDE + xx}

    def at_y(yy):
        return {"fs": z_lo * SIDE * SIDE + yy * SIDE + x}

    def at_z(zz):
        return {"rep": zz // 2, "fs": lax.rem(zz, 2) * SIDE * SIDE + y * SIDE + x}

    partner = {"tp": other}
    mesh_type = pl.DeviceIdType.MESH

    def remote(src, dst, send, recv, device):
        return pltpu.make_async_remote_copy(
            src_ref=src, dst_ref=dst, send_sem=send, recv_sem=recv, device_id=device, device_id_type=mesh_type
        )

    def of(ref, i, n):
        return pl.ds(pl.multiple_of(i * n, n), n)

    conv_row = z_lo * SIDE + y
    loads = [
        pltpu.make_async_copy(wv_hbm, conv_w.at[conv_row, of(0, x, k_rows), 0:channels], load_sem.at[0]),
        pltpu.make_async_copy(wg_hbm, conv_w.at[conv_row, of(0, x, k_rows), channels : 2 * channels], load_sem.at[1]),
        pltpu.make_async_copy(wb_hbm, conv_w.at[conv_row, of(0, x, k_rows), 2 * channels : 3 * channels], load_sem.at[2]),
        pltpu.make_async_copy(wu_hbm, up_w.at[y, :, of(0, x, block)], load_sem.at[3]),
        pltpu.make_async_copy(wd_hbm, down_w.at[y, of(0, x, block), :], load_sem.at[4]),
        pltpu.make_async_copy(x_hbm, x_full.at[:, of(0, core, half)], load_sem.at[5]),
    ]
    for load in loads:
        load.start()

    barrier = pltpu.get_barrier_semaphore()
    for device in (at_x(x_next), at_x(x_prev), at_y(y_next), at_y(y_prev), at_z(z_next), at_z(z_prev), partner):
        pl.semaphore_signal(barrier, inc=1, device_id=device, device_id_type=mesh_type)
    pl.semaphore_wait(barrier, 7)

    def span(first, size, part):
        return pl.ds(first, size) if part is None else pl.ds(first + part * (size // 2), size // 2)

    def conv_piece(first, width):
        def view(what, yy, xx, colour, part):
            cols = span(first + colour * width, width, part)
            if what == "block":
                return conv_w.at[z_lo * SIDE + yy, of(0, xx, k_rows), cols]
            if what == "row":
                return conv_w.at[z_lo * SIDE + yy, :, cols]
            return conv_w.at[pl.ds(z_lo * SIDE, SIDE), of(0, xx, k_rows), cols]

        return view

    def up_piece(index):
        size = features // UP_PIECES // 2

        def view(what, yy, xx, colour, part):
            depth = span((2 * index + colour) * size, size, part)
            if what == "block":
                return up_w.at[yy, depth, of(0, xx, block)]
            if what == "row":
                return up_w.at[yy, depth, :]
            return up_w.at[:, depth, of(0, xx, block)]

        return view

    width = half // DOWN_PIECES

    def down_piece(index):
        def view(what, yy, xx, colour, part):
            cols = span(colour * half + index * width, width, part)
            if what == "block":
                return down_w.at[yy, of(0, xx, block), cols]
            if what == "row":
                return down_w.at[yy, :, cols]
            return down_w.at[:, of(0, xx, block), cols]

        return view

    views = [conv_piece(0, channels), conv_piece(2 * channels, channels // 2)]
    views += [up_piece(i) for i in range(UP_PIECES)] + [down_piece(i) for i in range(DOWN_PIECES)]

    def step_copies(piece, step):
        view = views[piece]
        if step == 0:
            own = [("block", y, x, 0, None), ("block", y, x, 1, None)]
            pairs = [(own[0], own[0]), (own[1], own[1])]
        elif step == 1:
            pairs = [
                (("block", y, x_prev, 0, 0), ("block", y, x_next, 0, 1)),
                (("block", y_prev, x, 1, 0), ("block", y_next, x, 1, 1)),
            ]
        elif step == 2:
            pairs = [(("row", y, x, 0, None),) * 2, (("col", y, x, 1, None),) * 2]
        else:
            pairs = [
                (("row", y_prev, x, 0, 0), ("row", y_next, x, 0, 1)),
                (("col", y, x_prev, 1, 0), ("col", y, x_next, 1, 1)),
            ]
        along_x = (at_x(x_next), at_x(x_prev))
        along_y = (at_y(y_next), at_y(y_prev))
        copies = []
        for colour in range(2):
            devices = along_x if (step < 2) == (colour == 0) else along_y
            for way in range(2):
                ref = view(*pairs[colour][way])
                copies.append(
                    remote(
                        ref, ref,
                        send_sem.at[((piece * 4 + step) * 2 + colour) * 2 + way],
                        recv_sem.at[((piece * 4 + step) * 2 + colour) * 2 + way],
                        devices[way],
                    )
                )
        return copies

    flying = {}
    z_flying = {}

    def z_copies(piece, stage):
        view = views[piece]
        sets = {
            0: [(("row", y, x, 0, None), ("col", y, x, 1, None))],
            1: [
                (("row", y_prev, x, 0, None), ("col", y, x_prev, 1, None)),
                (("row", y_next, x, 0, None), ("col", y, x_next, 1, None)),
            ],
            2: [(("row", lax.rem(y + 2, SIDE), x, 0, None), ("col", y, lax.rem(x + 2, SIDE), 1, None))],
        }[stage]
        copies = []
        for number, pair in enumerate(sets):
            slot = {0: 0, 1: 1, 2: 3}[stage] + number
            for colour in range(2):
                ref = view(*pair[colour])
                index = (piece * 4 + slot) * 2 + colour
                copies.append(remote(ref, ref, z_send.at[index], z_recv.at[index], at_z((z_next, z_prev)[colour])))
        return copies

    def advance(piece):
        step = 0
        if piece in flying:
            step, copies = flying[piece]
            for copy in copies:
                copy.wait()
            step += 1
        if step < 4:
            copies = step_copies(piece, step)
            for copy in copies:
                copy.start()
            flying[piece] = (step, copies)
        if piece < 2 and step >= 2:
            copies = z_copies(piece, step - 2)
            for copy in copies:
                copy.start()
            z_flying.setdefault(piece, []).extend(copies)

    def z_wait(piece):
        for copy in z_flying[piece]:
            copy.wait()

    state = {"first": 0, "next": 2}

    def tick():
        for piece in range(state["first"], state["next"]):
            advance(piece)
        if state["next"] < PIECES:
            advance(state["next"])
            state["next"] += 1
        while state["first"] < state["next"] and flying[state["first"]][0] == 3 and state.get("done", {}).get(state["first"]):
            state["first"] += 1

    steps_done = [0] * PIECES

    def beat():
        for piece in range(PIECES):
            if 0 < steps_done[piece] <= 4:
                advance(piece)
                steps_done[piece] += 1
        for piece in range(PIECES):
            if steps_done[piece] == 0:
                advance(piece)
                steps_done[piece] = 1
                break

    x_swap = remote(x_hbm, x_full.at[:, of(0, core, half)], pair_send.at[0], pair_recv.at[0], partner)
    x_swap.start()
    loads[0].wait()
    loads[1].wait()
    beat()
    loads[2].wait()
    advance(1)
    steps_done[1] = 1
    loads[3].wait()
    loads[4].wait()
    advance(2)
    steps_done[2] = 1

    def rms(src, dst, gain, first, count, step_rows=32):
        scale = gain[...]

        def body(i, carry):
            at = pl.ds(pl.multiple_of(first + i * step_rows, step_rows), step_rows)
            values = src[at, :].astype(F32)
            mean = jnp.sum(values * values, axis=1, keepdims=True) * (1.0 / features)
            dst[at, :] = (values * lax.rsqrt(mean + 1e-6) * scale).astype(BF16)
            return carry

        lax.fori_loop(0, count // step_rows, body, 0)

    loads[5].wait()
    x_swap.wait()
    rms(x_full, normed, mix_gain, 0, rows)
    beat()
    beat()
    beat()
    padded[:, 0:32, :] = jnp.zeros((sequences, 32, channels), F32)
    beat()
    z_wait(0)

    tile = 256
    for n in range(channels // tile):
        cols = slice(n * tile, (n + 1) * tile)
        gcols = slice(channels + n * tile, channels + (n + 1) * tile)
        value = jnp.dot(normed[0:rows, :], conv_w[:, :, cols].reshape(features, tile), preferred_element_type=F32)
        gate = jnp.dot(normed[0:rows, :], conv_w[:, :, gcols].reshape(features, tile), preferred_element_type=F32)
        gated = value * jax.nn.sigmoid(gate)
        padded[:, 32 : 32 + LEN, cols] = gated.reshape(sequences, LEN, tile)
    beat()

    def filter_body(s, carry):
        at = pl.ds(pl.multiple_of(s * LEN, LEN), LEN)
        first = jnp.zeros((LEN, 128), F32)
        square = jnp.zeros((LEN, 128), F32)
        for lane in range(channels // 128):
            cols = slice(lane * 128, (lane + 1) * 128)
            slab = padded[s, :, cols]
            total = jnp.broadcast_to(conv_bias[:, cols], (LEN, 128))
            for shift in range(8):
                acc = None
                for q in range(5):
                    k = 8 * q + shift - 2
                    if 0 <= k < KW:
                        high = LEN + (8 if shift else 0)
                        term = taps[k : k + 1, cols] * slab[8 * q : 8 * q + high]
                        acc = term if acc is None else acc + term
                total = total + acc[shift : shift + LEN]
            filtered[at, cols] = total
            first = first + total
            square = square + total * total
        stat_own[0, at, :] = first
        stat_own[1, at, :] = square
        return carry

    lax.fori_loop(0, sequences, filter_body, 0)
    stat_swap = remote(stat_own, stat_got, pair_send.at[1], pair_recv.at[1], partner)
    stat_swap.start()
    beat()
    stat_swap.wait()

    def norm_body(i, carry):
        at = pl.ds(pl.multiple_of(i * 64, 64), 64)
        scale = 1.0 / (2 * channels)
        mean = jnp.sum(stat_own[0, at, :] + stat_got[0, at, :], axis=1, keepdims=True) * scale
        power = jnp.sum(stat_own[1, at, :] + stat_got[1, at, :], axis=1, keepdims=True) * scale
        spread = lax.rsqrt(power - mean * mean + 1e-5)
        centred = (filtered[at, :] - mean) * spread * chan_gain[...] + chan_bias[...]
        act[at, :] = (centred * jax.nn.sigmoid(centred)).astype(BF16)
        return carry

    lax.fori_loop(0, rows // 64, norm_body, 0)
    z_wait(1)

    def back_half(which):
        weights = conv_w[pl.ds(which * SIDE, SIDE), :, 2 * channels : 3 * channels].reshape(half, channels)
        return lax.dot_general(act[...], weights, (((1,), (1,)), ((), ())), preferred_element_type=F32)

    mix_send[...] = back_half(other).astype(BF16)
    mix_swap = remote(mix_send, mix_got, pair_send.at[2], pair_recv.at[2], partner)
    mix_swap.start()
    own_sum[...] = back_half(core)
    beat()
    mix_swap.wait()
    mine = of(0, core, half)
    mixed = own_sum[...].astype(BF16).astype(F32) + mix_got[...].astype(F32)
    second[0:rows, mine] = (x_full[:, mine].astype(F32) + mixed).astype(BF16)

    own_rows = second.at[0:rows, mine]
    second_swap = remote(own_rows, own_rows, pair_send.at[3], pair_recv.at[3], partner)
    low, high = pl.ds(0, part_rows), pl.ds(part_rows, part_rows)
    from_prev, from_next = pl.ds(rows, part_rows), pl.ds(rows + part_rows, part_rows)
    hops = [
        remote(second.at[low, mine], second.at[from_prev, mine], hop_send.at[0], hop_recv.at[0], at_z(z_next)),
        remote(second.at[high, mine], second.at[from_next, mine], hop_send.at[1], hop_recv.at[1], at_z(z_prev)),
    ]
    for hop in hops:
        hop.start()
    second_swap.start()
    beat()
    second_swap.wait()

    def up(first):
        at = pl.ds(first, rows)

        def body(i, carry):
            product = jnp.dot(normed[at, :], up_w[i], preferred_element_type=F32)
            positive = jnp.maximum(product, 0.0)
            hidden[at, pl.ds(pl.multiple_of(i * SIDE * block, SIDE * block), SIDE * block)] = (positive * positive).astype(BF16)
            return carry

        lax.fori_loop(0, SIDE, body, 0)

    rms(second, normed, feed_gain, 0, rows)
    up(0)
    for hop in hops:
        hop.wait()
    foreign = second.at[pl.ds(rows, rows), mine]
    foreign_swap = remote(foreign, foreign, pair_send.at[4], pair_recv.at[4], partner)
    foreign_swap.start()
    beat()
    foreign_swap.wait()
    rms(second, normed, feed_gain, rows, rows)
    up(rows)
    beat()

    def down(index):
        def product(which, first):
            cols = pl.ds(pl.multiple_of(which * half + index * width, width), width)
            weights = down_w[:, :, cols].reshape(SIDE * SIDE * block, width)
            return jnp.dot(hidden[pl.ds(first, rows), :], weights, preferred_element_type=F32)

        cols = pl.ds(index * width, width)
        for first in (0, rows):
            part_send[pl.ds(first, rows), cols] = product(other, first).astype(BF16)
        swap = remote(part_send.at[:, cols], part_got.at[:, cols], pair_send.at[5 + index], pair_recv.at[5 + index], partner)
        swap.start()
        for first in (rows, 0):
            keep[pl.ds(first, rows), :] = product(core, first)
        swap.wait()
        ret_send[:, cols] = (keep[pl.ds(rows, rows), :] + part_got[pl.ds(rows, rows), cols].astype(F32)).astype(BF16)
        back = [
            remote(ret_send.at[low, cols], ret_got.at[low, cols], hop_send.at[2 + 2 * index], hop_recv.at[2 + 2 * index], at_z(z_prev)),
            remote(ret_send.at[high, cols], ret_got.at[high, cols], hop_send.at[3 + 2 * index], hop_recv.at[3 + 2 * index], at_z(z_next)),
        ]
        for copy in back:
            copy.start()
        own_sum[:, cols] = keep[pl.ds(0, rows), :] + part_got[pl.ds(0, rows), cols].astype(F32)
        return back

    outs = []

    def finish(index, back):
        for copy in back:
            copy.wait()
        cols = pl.ds(index * width, width)
        there = pl.ds(pl.multiple_of(core * half + index * width, width), width)
        total = second[0:rows, there].astype(F32) + own_sum[:, cols] + ret_got[:, cols].astype(F32)
        out_vmem[:, cols] = total.astype(BF16)
        copy = pltpu.make_async_copy(out_vmem.at[:, cols], out_hbm.at[:, cols], out_sem.at[index])
        copy.start()
        outs.append(copy)

    waiting = None
    for index in range(DOWN_PIECES):
        while steps_done[2 + UP_PIECES + index] < 5:
            beat()
        back = down(index)
        if waiting is not None:
            finish(index - 1, waiting)
        waiting = back
    finish(DOWN_PIECES - 1, waiting)
    for copy in outs:
        copy.wait()


def shards(
    hidden_in, mix_gain, w_value, w_gate, conv_taps, conv_bias, chan_gain, chan_bias, w_back, feed_gain, w_up, w_down
):
    rows, half = hidden_in.shape
    features = 2 * half
    channels = w_value.shape[1]
    block = w_up.shape[1]
    plane = SIDE * SIDE
    sequences = rows // LEN
    vmem = pl.BlockSpec(memory_space=pltpu.VMEM)
    hbm = pl.BlockSpec(memory_space=pl.ANY)
    dma = pltpu.SemaphoreType.DMA
    width = half // DOWN_PIECES
    scratch = [
        pltpu.VMEM((2 * SIDE, SIDE * w_value.shape[0], 3 * channels), BF16),
        pltpu.VMEM((SIDE, features, SIDE * block), BF16),
        pltpu.VMEM((SIDE, SIDE * block, features), BF16),
        pltpu.VMEM((rows, features), BF16),
        pltpu.VMEM((2 * rows, features), BF16),
        pltpu.VMEM((sequences, 32 + LEN, channels), F32),
        pltpu.VMEM((rows, channels), F32),
        pltpu.VMEM((rows, channels), BF16),
        pltpu.VMEM((2, rows, 128), F32),
        pltpu.VMEM((2, rows, 128), F32),
        pltpu.VMEM((rows, half), BF16),
        pltpu.VMEM((rows, half), BF16),
        pltpu.VMEM((2 * rows, features), BF16),
        pltpu.VMEM((2 * rows, plane * block), BF16),
        pltpu.VMEM((2 * rows, half), BF16),
        pltpu.VMEM((2 * rows, half), BF16),
        pltpu.VMEM((2 * rows, width), F32),
        pltpu.VMEM((rows, half), F32),
        pltpu.VMEM((rows, half), BF16),
        pltpu.VMEM((rows, half), BF16),
        pltpu.VMEM((rows, half), BF16),
        dma((6,)),
        dma((PIECES * 16,)),
        dma((PIECES * 16,)),
        dma((16,)),
        dma((16,)),
        dma((5 + DOWN_PIECES,)),
        dma((5 + DOWN_PIECES,)),
        dma((2 + 2 * DOWN_PIECES,)),
        dma((2 + 2 * DOWN_PIECES,)),
        dma((DOWN_PIECES,)),
    ]
    return pl.pallas_call(
        kernel,
        out_shape=jax.ShapeDtypeStruct((rows, half), BF16),
        in_specs=[hbm, vmem, hbm, hbm, vmem, vmem, vmem, vmem, hbm, vmem, hbm, hbm],
        out_specs=hbm,
        scratch_shapes=scratch,
        compiler_params=pltpu.CompilerParams(
            collective_id=0, has_side_effects=True, vmem_limit_bytes=67043328
        ),
    )(
        hidden_in,
        mix_gain[None, :],
        w_value,
        w_gate,
        conv_taps,
        conv_bias[None, :],
        chan_gain[None, :],
        chan_bias[None, :],
        w_back.T,
        feed_gain[None, :],
        w_up,
        w_down,
    )


def solution(mesh):
    placed = (
        P(("rep", "fs"), "tp"),
        P(),
        P("fs", "tp"),
        P("fs", "tp"),
        P(None, "tp"),
        P("tp"),
        P("tp"),
        P("tp"),
        P("tp", "fs"),
        P(),
        P(None, ("fs", "tp")),
        P(("fs", "tp"), None),
    )
    return jax.shard_map(
        shards, mesh=mesh, in_specs=placed, out_specs=P(("rep", "fs"), "tp"), check_vma=False
    )
```

time: 709 us -> 146 us (0.21)
  waiting for transfers between devices: 555 us -> 0 us
  Pallas kernels: 0 us -> 143 us
  blocking collectives: 64.1 us -> 0 us
  matrix products: 42.7 us -> 0 us
  other arithmetic: 17 us -> 0 us
  between operations: 13.3 us -> 0.01 us
  starting transfers between devices: 8.94 us -> 0 us
    all_gather x4 -> x0, waiting for transfers between devices: 554 us -> none  [the longest x1 223 us: shards(): lax.all_gather(w_up, 'fs', axis=1, tiled=True)]
    pallas_call x0 -> x1, Pallas kernels: none -> 143 us  [shards(): pl.pallas_call(kernel, out_shape=jax.ShapeDtypeStruct((rows, half), BF16)...]
    dot_general x4 -> x0, matrix products: 42.7 us -> none  [the longest x1 33.8 us: shards(): jnp.dot(hidden, lax.all_gather(w_down, 'fs', axis=0, tiled=True), preferr...]
    all_to_all x3 -> x0, blocking collectives: 42 us -> none  [the longest x2 35.1 us: summed_on_arrival(): parts = lax.all_to_all(in_blocks(array, dim, count), axis, 0, 0, tiled=True)]
    psum x1 -> x0, blocking collectives: 22.1 us -> none  [shards(): lax.psum((jnp.sum(filtered, axis=1), jnp.sum(filtered * filtered, axis=1)...]
    reduce_sum x5 -> x0, other arithmetic: 9.67 us -> none  [the longest x1 5.47 us: shards(): jnp.sum(filtered, axis=1)]
    all_to_all x1 -> x0, starting transfers between devices: 8.63 us -> none  [copy_for_each(): return lax.all_to_all(copies, axis, split_axis=0, concat_axis=0, tiled=True)]
  transfers between devices with their start and end apart: 5 -> 0, of which waited for: 4 -> 0; matrix products, arithmetic and copies ran while one was open for 3% -> 0% of each run, Pallas kernels for 0% -> 0%
where the time goes in v1:
time: 146 us
  Pallas kernels  143 us (98%)
  local copies, waits for them, and re-layouts  2.47 us (2%)
    pallas_call x1, Pallas kernels, shards(): pl.pallas_call(kernel, out_shape=jax.ShapeDtypeStruct((rows, half), BF16)...  143 us

profile of v1, /device:TPU:1, one launch (start us, length us, event | category | flops | bytes accessed | tf_op | source)
XLA Modules:
  0.0 145.6 jit_solution(5201480859123143620)
XLA Ops:
  0.0 143.1 %shard_map.118 = bf16[640,1024]{1,0:T(8,128)(2,1)} custom-call(bf16[640,1024]{1,0:T(8,128)(2,1)} %x_hbm.1, f32[1,2048]{1,0:T(1,128)} %bitcast.7, bf16[64,512]{1,0:T(8,128)(2,1)} %wv_hbm.1, bf16[64,512]{1,0:T(8,128)(2,1)} %wg_hbm.1, f32[31,512]{1,0:T(8,128)} %taps.1, f32[1,512]{1,0:T(1,128)} %bitcast.9, f32[1,512]{1,0:T(1,128)} %bitcast.10, ...), custom_call_target="tpu_custom_call" | custom-call | tf_op jit(solution)/shard_map/pallas_call | solution.py:465
  143.1 2.5 %copy.14 = bf16[640,1024]{1,0:T(8,128)(2,1)} copy(bf16[640,1024]{1,0:T(8,128)(2,1)} %shard_map.118) | data formatting | bytes 2621440

commit v2 on v1

v2 whole, which is shorter than its diff:
```python
import functools

import jax
import jax.numpy as jnp
from jax import lax
from jax.experimental import pallas as pl
from jax.experimental.pallas import tpu as pltpu
from jax.sharding import PartitionSpec as P

KW = 31
LEN = 128
SIDE = 4
F32 = jnp.float32
BF16 = jnp.bfloat16
UP_PIECES = 4
DOWN_WIDTHS = (256, 256, 128, 128, 128, 128)
DOWN_FIRST = (0, 256, 512, 640, 768, 896)
DOWN_PIECES = len(DOWN_WIDTHS)
PIECES = 2 + UP_PIECES + DOWN_PIECES
UNITS = (1, 0.5) + (4 / UP_PIECES,) * UP_PIECES + tuple(width / 256 for width in DOWN_WIDTHS)

ORDER = (
    "a1", "a0", "a3", "a2", "a7", "a0", "a1", "a10", "a5", "rmsx", "a4", "a6", "a0", "a9", "a3", "a1", "z00", "a4",
    "a0", "z10", "a5", "a2", "a8", "a6", "a3", "a1", "a11", "z01", "a5", "a2", "a4", "a7", "a0", "z02", "vg0", "a1",
    "z11", "a9", "a11", "a3", "zw0", "a5", "z12", "vg1", "filter", "a2", "statw", "chan", "a4", "zw1", "a8", "bo",
    "bw", "a7", "mixw", "second", "a2", "a10", "secw", "a5", "a6", "a4", "rms", "a3", "a8", "upa", "upb", "a7",
    "hopw", "a6", "forw", "rmsf", "a9", "a8", "a10", "upfa", "a7", "upfb", "a6", "a11", "down0", "a9", "down1", "a8",
    "a10", "down2", "a11", "a9", "down3", "a10", "down4", "a11", "down5",
)


def kernel(
    x_hbm, mix_gain, wv_hbm, wg_hbm, taps, conv_bias, chan_gain, chan_bias, wb_hbm, feed_gain, wu_hbm, wd_hbm,
    out_hbm,
    conv_w, up_w, down_w, x_full, normed, padded, filtered, act, stat_own, stat_got,
    second, hidden, part, part_got, own_sum, ret_send, ret_got, out_vmem,
    load_sem, send_sem, recv_sem, z_send, z_recv, pair_send, pair_recv, hop_send, hop_recv, out_sem,
):
    rows, half = x_hbm.shape
    features = 2 * half
    channels = wv_hbm.shape[1]
    k_rows = wv_hbm.shape[0]
    block = wu_hbm.shape[1]
    sequences = rows // LEN
    part_rows = rows // 2

    core = lax.axis_index("tp")
    other = 1 - core
    place = lax.axis_index("fs")
    z_hi = lax.axis_index("rep")
    x = lax.rem(place, SIDE)
    y = lax.rem(place // SIDE, SIDE)
    z_lo = place // (SIDE * SIDE)
    z = z_hi * 2 + z_lo
    x_next, x_prev = lax.rem(x + 1, SIDE), lax.rem(x + SIDE - 1, SIDE)
    y_next, y_prev = lax.rem(y + 1, SIDE), lax.rem(y + SIDE - 1, SIDE)
    z_next, z_prev = lax.rem(z + 1, 4), lax.rem(z + 3, 4)

    def at_x(xx):
        return {"fs": z_lo * SIDE * SIDE + y * SIDE + xx}

    def at_y(yy):
        return {"fs": z_lo * SIDE * SIDE + yy * SIDE + x}

    def at_z(zz):
        return {"rep": zz // 2, "fs": lax.rem(zz, 2) * SIDE * SIDE + y * SIDE + x}

    partner = {"tp": other}
    mesh_type = pl.DeviceIdType.MESH

    def remote(src, dst, send, recv, device):
        return pltpu.make_async_remote_copy(
            src_ref=src, dst_ref=dst, send_sem=send, recv_sem=recv, device_id=device, device_id_type=mesh_type
        )

    def of(ref, i, n):
        return pl.ds(pl.multiple_of(i * n, n), n)

    conv_row = z_lo * SIDE + y
    loads = [
        pltpu.make_async_copy(wv_hbm, conv_w.at[conv_row, of(0, x, k_rows), 0:channels], load_sem.at[0]),
        pltpu.make_async_copy(wg_hbm, conv_w.at[conv_row, of(0, x, k_rows), channels : 2 * channels], load_sem.at[1]),
        pltpu.make_async_copy(wb_hbm, conv_w.at[conv_row, of(0, x, k_rows), 2 * channels : 3 * channels], load_sem.at[2]),
        pltpu.make_async_copy(wu_hbm, up_w.at[y, :, of(0, x, block)], load_sem.at[3]),
        pltpu.make_async_copy(x_hbm, x_full.at[:, of(0, core, half)], load_sem.at[4]),
    ]
    for index in range(DOWN_PIECES):
        width, first = DOWN_WIDTHS[index], DOWN_FIRST[index]
        for h in range(2):
            src = wd_hbm.at[:, pl.ds(h * half + first, width)]
            dst = down_w.at[y, of(0, x, block), pl.ds(2 * first + h * width, width)]
            loads.append(pltpu.make_async_copy(src, dst, load_sem.at[5]))
    for load in loads:
        load.start()

    barrier = pltpu.get_barrier_semaphore()
    for device in (at_x(x_next), at_x(x_prev), at_y(y_next), at_y(y_prev), at_z(z_next), at_z(z_prev), partner):
        pl.semaphore_signal(barrier, inc=1, device_id=device, device_id_type=mesh_type)
    with jax.named_scope("barrier"):
        pl.semaphore_wait(barrier, 7)

    def span(first, size, part):
        return pl.ds(first, size) if part is None else pl.ds(first + part * (size // 2), size // 2)

    def conv_piece(first, width):
        def view(what, yy, xx, colour, part):
            cols = span(first + colour * width, width, part)
            if what == "block":
                return conv_w.at[z_lo * SIDE + yy, of(0, xx, k_rows), cols]
            if what == "row":
                return conv_w.at[z_lo * SIDE + yy, :, cols]
            return conv_w.at[pl.ds(z_lo * SIDE, SIDE), of(0, xx, k_rows), cols]

        return view

    def up_piece(index):
        size = features // UP_PIECES // 2

        def view(what, yy, xx, colour, part):
            depth = span((2 * index + colour) * size, size, part)
            if what == "block":
                return up_w.at[yy, depth, of(0, xx, block)]
            if what == "row":
                return up_w.at[yy, depth, :]
            return up_w.at[:, depth, of(0, xx, block)]

        return view

    def down_piece(index):
        width, first = DOWN_WIDTHS[index], DOWN_FIRST[index]

        def view(what, yy, xx, colour, part):
            cols = pl.ds(2 * first + colour * width, width)
            size = block if part is None else block // 2
            rows_of_block = pl.ds(pl.multiple_of(xx * block + (part or 0) * size, size), size)
            if what == "block":
                return down_w.at[yy, rows_of_block, cols]
            if what == "row":
                return down_w.at[yy, span(0, SIDE * block, part), cols]
            return down_w.at[:, rows_of_block, cols]

        return view

    views = [conv_piece(0, channels), conv_piece(2 * channels, channels // 2)]
    views += [up_piece(i) for i in range(UP_PIECES)] + [down_piece(i) for i in range(DOWN_PIECES)]

    def step_copies(piece, step):
        view = views[piece]
        if step == 0:
            own = [("block", y, x, 0, None), ("block", y, x, 1, None)]
            pairs = [(own[0], own[0]), (own[1], own[1])]
        elif step == 1:
            pairs = [
                (("block", y, x_prev, 0, 0), ("block", y, x_next, 0, 1)),
                (("block", y_prev, x, 1, 0), ("block", y_next, x, 1, 1)),
            ]
        elif step == 2:
            pairs = [(("row", y, x, 0, None),) * 2, (("col", y, x, 1, None),) * 2]
        else:
            pairs = [
                (("row", y_prev, x, 0, 0), ("row", y_next, x, 0, 1)),
                (("col", y, x_prev, 1, 0), ("col", y, x_next, 1, 1)),
            ]
        along_x = (at_x(x_next), at_x(x_prev))
        along_y = (at_y(y_next), at_y(y_prev))
        copies = []
        for colour in range(2):
            devices = along_x if (step < 2) == (colour == 0) else along_y
            for way in range(2):
                ref = view(*pairs[colour][way])
                copies.append(remote(ref, ref, send_sem.at[piece], recv_sem.at[piece * 4 + step], devices[way]))
        return copies

    flying = {}

    def z_copies(piece, stage):
        view = views[piece]
        sets = {
            0: [(("row", y, x, 0, None), ("col", y, x, 1, None))],
            1: [
                (("row", y_prev, x, 0, None), ("col", y, x_prev, 1, None)),
                (("row", y_next, x, 0, None), ("col", y, x_next, 1, None)),
            ],
            2: [(("row", lax.rem(y + 2, SIDE), x, 0, None), ("col", y, lax.rem(x + 2, SIDE), 1, None))],
        }[stage]
        copies = []
        for pair in sets:
            for colour in range(2):
                ref = view(*pair[colour])
                copies.append(remote(ref, ref, z_send.at[piece], z_recv.at[piece], at_z((z_next, z_prev)[colour])))
        return copies

    counts = {}

    def advance(piece):
        counts[piece] = counts.get(piece, 0) + 1
        step = 0
        if piece in flying:
            step = flying[piece]
            with jax.named_scope(f"wait_{piece}_{step}"):
                kib = int(4 * UNITS[piece] * 64 * (1, 0.5, 4, 2)[step])
                four = up_w.at[0, 0:kib, :]
                pltpu.make_async_copy(four, four, recv_sem.at[piece * 4 + step]).wait()
                pltpu.make_async_copy(four, four, send_sem.at[piece]).wait()
            step += 1
        if step < 4:
            copies = step_copies(piece, step)
            for copy in copies:
                copy.start()
            flying[piece] = step

    def z_go(piece, stage):
        for copy in z_copies(piece, stage):
            copy.start()

    def z_wait(piece):
        first = 2 * channels * piece
        whole = conv_w.at[pl.ds((1 - z_lo) * SIDE, SIDE), :, pl.ds(first, (2 - piece) * channels)]
        pltpu.make_async_copy(whole, whole, z_recv.at[piece]).wait()
        pltpu.make_async_copy(whole, whole, z_send.at[piece]).wait()

    ups = list(range(2, 2 + UP_PIECES))
    downs = list(range(2 + UP_PIECES, PIECES))

    def rms(src, dst, gain, first, count, step_rows=32):
        scale = gain[...]

        def body(i, carry):
            at = pl.ds(pl.multiple_of(first + i * step_rows, step_rows), step_rows)
            values = src[at, :].astype(F32)
            mean = jnp.sum(values * values, axis=1, keepdims=True) * (1.0 / features)
            dst[at, :] = (values * lax.rsqrt(mean + 1e-6) * scale).astype(BF16)
            return carry

        lax.fori_loop(0, count // step_rows, body, 0)

    mine = of(0, core, half)
    own, foreign = pl.ds(0, rows), pl.ds(rows, rows)
    low, high = pl.ds(0, part_rows), pl.ds(part_rows, part_rows)
    from_prev, from_next = pl.ds(rows, part_rows), pl.ds(rows + part_rows, part_rows)
    mix_send, mix_got = part.at[0, 0:rows, :], part_got.at[0:rows, :]
    x_swap = remote(x_hbm, x_full.at[:, mine], pair_send.at[0], pair_recv.at[0], partner)
    stat_swap = remote(stat_own, stat_got, pair_send.at[1], pair_recv.at[1], partner)
    mix_swap = remote(mix_send, mix_got, pair_send.at[2], pair_recv.at[2], partner)
    second_swap = remote(second.at[own, mine], second.at[own, mine], pair_send.at[3], pair_recv.at[3], partner)
    foreign_swap = remote(second.at[foreign, mine], second.at[foreign, mine], pair_send.at[4], pair_recv.at[4], partner)
    hops = [
        remote(second.at[low, mine], second.at[from_prev, mine], hop_send.at[0], hop_recv.at[0], at_z(z_next)),
        remote(second.at[high, mine], second.at[from_next, mine], hop_send.at[0], hop_recv.at[0], at_z(z_prev)),
    ]

    def first_norm():
        loads[4].wait()
        x_swap.wait()
        rms(x_full, normed, mix_gain, 0, rows)
        padded[:, 0:32, :] = jnp.zeros((sequences, 32, channels), F32)

    tile = 256

    def plane_dot(which, cols):
        at = pl.ds(pl.multiple_of(which * half, half), half)
        weights = conv_w[pl.ds(which * SIDE, SIDE), :, cols].reshape(half, tile)
        return jnp.dot(normed[0:rows, at], weights, preferred_element_type=F32)

    def value_gate_own():
        for n in range(2 * channels // tile):
            cols = slice(n * tile, (n + 1) * tile)
            own_sum[:, cols] = plane_dot(z_lo, cols)

    def value_gate_rest():
        for n in range(channels // tile):
            cols = slice(n * tile, (n + 1) * tile)
            gcols = slice(channels + n * tile, channels + (n + 1) * tile)
            value = own_sum[:, cols] + plane_dot(1 - z_lo, cols)
            gate = own_sum[:, gcols] + plane_dot(1 - z_lo, gcols)
            gated = value * jax.nn.sigmoid(gate)
            padded[:, 32 : 32 + LEN, cols] = gated.reshape(sequences, LEN, tile)

    def causal_filter():
        def body(s, carry):
            at = pl.ds(pl.multiple_of(s * LEN, LEN), LEN)
            first = jnp.zeros((LEN, 128), F32)
            square = jnp.zeros((LEN, 128), F32)
            for lane in range(channels // 128):
                cols = slice(lane * 128, (lane + 1) * 128)
                slab = padded[s, :, cols]
                total = jnp.broadcast_to(conv_bias[:, cols], (LEN, 128))
                for shift in range(8):
                    acc = None
                    for q in range(5):
                        k = 8 * q + shift - 2
                        if 0 <= k < KW:
                            tall = LEN + (8 if shift else 0)
                            term = taps[k : k + 1, cols] * slab[8 * q : 8 * q + tall]
                            acc = term if acc is None else acc + term
                    total = total + acc[shift : shift + LEN]
                filtered[at, cols] = total
                first = first + total
                square = square + total * total
            stat_own[0, at, :] = first
            stat_own[1, at, :] = square
            return carry

        lax.fori_loop(0, sequences, body, 0)
        stat_swap.start()

    def channel_norm():
        def body(i, carry):
            at = pl.ds(pl.multiple_of(i * 64, 64), 64)
            scale = 1.0 / (2 * channels)
            mean = jnp.sum(stat_own[0, at, :] + stat_got[0, at, :], axis=1, keepdims=True) * scale
            power = jnp.sum(stat_own[1, at, :] + stat_got[1, at, :], axis=1, keepdims=True) * scale
            spread = lax.rsqrt(power - mean * mean + 1e-5)
            centred = (filtered[at, :] - mean) * spread * chan_gain[...] + chan_bias[...]
            act[at, :] = (centred * jax.nn.sigmoid(centred)).astype(BF16)
            return carry

        lax.fori_loop(0, rows // 64, body, 0)

    def back_half(which):
        weights = conv_w[pl.ds(which * SIDE, SIDE), :, 2 * channels : 3 * channels].reshape(half, channels)
        return lax.dot_general(act[...], weights, (((1,), (1,)), ((), ())), preferred_element_type=F32)

    def back_other():
        mix_send[...] = back_half(other).astype(BF16)
        mix_swap.start()

    def back_own():
        own_sum[...] = back_half(core)

    def residual():
        mixed = own_sum[...].astype(BF16).astype(F32) + mix_got[...].astype(F32)
        second[own, mine] = (x_full[:, mine].astype(F32) + mixed).astype(BF16)
        for hop in hops:
            hop.start()
        second_swap.start()

    def up(first, begin, end):
        at = pl.ds(first, rows)

        def body(i, carry):
            product = jnp.dot(normed[at, :], up_w[i], preferred_element_type=F32)
            positive = jnp.maximum(product, 0.0)
            hidden[at, pl.ds(pl.multiple_of(i * SIDE * block, SIDE * block), SIDE * block)] = (positive * positive).astype(BF16)
            return carry

        lax.fori_loop(begin, end, body, 0)

    def arrived():
        both = second.at[foreign, mine]
        pltpu.make_async_copy(both, both, hop_recv.at[0]).wait()
        pltpu.make_async_copy(both, both, hop_send.at[0]).wait()
        foreign_swap.start()

    swaps = {}

    def down(index):
        width, first = DOWN_WIDTHS[index], DOWN_FIRST[index]
        cols = pl.ds(first, width)
        depth = SIDE * SIDE * block
        swaps[index] = []
        for number, at in enumerate((foreign, own)):

            def body(i, carry):
                chunk = pl.ds(pl.multiple_of(at.start + i * part_rows, part_rows), part_rows)
                weights = down_w[:, :, pl.ds(2 * first, 2 * width)].reshape(depth, 2 * width)
                product = jnp.dot(hidden[chunk, :], weights, preferred_element_type=F32).astype(BF16)
                part[0, chunk, cols] = product[:, :width]
                part[1, chunk, cols] = product[:, width:]
                return carry

            lax.fori_loop(0, 2, body, 0)
            slot = 5 + 2 * index + number
            swap = remote(part.at[other, at, cols], part_got.at[at, cols], pair_send.at[5 if number == 0 else 6 + index % 2], pair_recv.at[slot], partner)
            swap.start()
            swaps[index].append(swap)

    def send_back(index):
        width, first = DOWN_WIDTHS[index], DOWN_FIRST[index]
        cols = pl.ds(first, width)
        swaps[index][0].wait()
        ret_send[:, cols] = (part[core, foreign, cols].astype(F32) + part_got[foreign, cols].astype(F32)).astype(BF16)
        for at, device in ((low, at_z(z_prev)), (high, at_z(z_next))):
            slot = 1 + index
            back = remote(ret_send.at[at, cols], ret_got.at[at, cols], hop_send.at[slot], hop_recv.at[slot], device)
            back.start()

    def sum_own(index):
        width, first = DOWN_WIDTHS[index], DOWN_FIRST[index]
        cols = pl.ds(first, width)
        swaps[index][1].wait()
        there = pl.ds(pl.multiple_of(core * half + first, 128), width)
        own_sum[:, cols] = (
            second[own, there].astype(F32) + part[core, own, cols].astype(F32) + part_got[own, cols].astype(F32)
        )

    def finish(index):
        width, first = DOWN_WIDTHS[index], DOWN_FIRST[index]
        cols = pl.ds(first, width)
        both = ret_got.at[:, cols]
        pltpu.make_async_copy(both, both, hop_recv.at[1 + index]).wait()
        pltpu.make_async_copy(both, both, hop_send.at[1 + index]).wait()
        out_vmem[:, cols] = (own_sum[:, cols] + ret_got[:, cols].astype(F32)).astype(BF16)
        copy = pltpu.make_async_copy(out_vmem.at[:, cols], out_hbm.at[:, cols], out_sem.at[0])
        copy.start()

    def down_step(index):
        down(index)
        send_back(index)
        if index:
            sum_own(index - 1)
        if index > 1:
            finish(index - 2)

    actions = dict(
        rmsx=first_norm,
        vg0=value_gate_own,
        zw0=lambda: z_wait(0),
        vg1=value_gate_rest,
        filter=causal_filter,
        statw=stat_swap.wait,
        chan=channel_norm,
        zw1=lambda: z_wait(1),
        bo=back_other,
        bw=back_own,
        mixw=mix_swap.wait,
        second=residual,
        secw=second_swap.wait,
        rms=lambda: rms(second, normed, feed_gain, 0, rows),
        upa=lambda: up(0, 0, SIDE // 2),
        upb=lambda: up(0, SIDE // 2, SIDE),
        hopw=arrived,
        forw=foreign_swap.wait,
        rmsf=lambda: rms(second, normed, feed_gain, rows, rows),
        upfa=lambda: up(rows, 0, SIDE // 2),
        upfb=lambda: up(rows, SIDE // 2, SIDE),
    )
    for index in range(DOWN_PIECES):
        actions[f"down{index}"] = functools.partial(down_step, index)

    first_load = {0: (0, 1), 1: (2,)}
    first_load.update({piece: (3,) for piece in ups})
    first_load.update({piece: (5,) for piece in downs})
    whole_down = down_w.at[y, of(0, x, block), :]
    loads[5:] = [pltpu.make_async_copy(whole_down, whole_down, load_sem.at[5])]
    loaded = set()

    x_swap.start()
    for name in ORDER:
        if name[0] == "a" and name[1:].isdigit():
            piece = int(name[1:])
            for number in first_load[piece]:
                if number not in loaded:
                    loads[number].wait()
                    loaded.add(number)
            advance(piece)
        elif name[0] == "z" and name[1:].isdigit():
            z_go(int(name[1]), int(name[2]))
        else:
            with jax.named_scope(name):
                actions[name]()

    sum_own(DOWN_PIECES - 1)
    finish(DOWN_PIECES - 2)
    with jax.named_scope("last"):
        finish(DOWN_PIECES - 1)
        pltpu.make_async_copy(out_vmem, out_hbm, out_sem.at[0]).wait()
    assert all(counts[piece] == 5 for piece in range(PIECES)), counts


def shards(
    hidden_in, mix_gain, w_value, w_gate, conv_taps, conv_bias, chan_gain, chan_bias, w_back, feed_gain, w_up, w_down
):
    rows, half = hidden_in.shape
    features = 2 * half
    channels = w_value.shape[1]
    block = w_up.shape[1]
    plane = SIDE * SIDE
    sequences = rows // LEN
    vmem = pl.BlockSpec(memory_space=pltpu.VMEM)
    hbm = pl.BlockSpec(memory_space=pl.ANY)
    dma = pltpu.SemaphoreType.DMA
    scratch = [
        pltpu.VMEM((2 * SIDE, SIDE * w_value.shape[0], 3 * channels), BF16),
        pltpu.VMEM((SIDE, features, SIDE * block), BF16),
        pltpu.VMEM((SIDE, SIDE * block, features), BF16),
        pltpu.VMEM((rows, features), BF16),
        pltpu.VMEM((2 * rows, features), BF16),
        pltpu.VMEM((sequences, 32 + LEN, channels), F32),
        pltpu.VMEM((rows, channels), F32),
        pltpu.VMEM((rows, channels), BF16),
        pltpu.VMEM((2, rows, 128), F32),
        pltpu.VMEM((2, rows, 128), F32),
        pltpu.VMEM((2 * rows, features), BF16),
        pltpu.VMEM((2 * rows, plane * block), BF16),
        pltpu.VMEM((2, 2 * rows, half), BF16),
        pltpu.VMEM((2 * rows, half), BF16),
        pltpu.VMEM((rows, half), F32),
        pltpu.VMEM((rows, half), BF16),
        pltpu.VMEM((rows, half), BF16),
        pltpu.VMEM((rows, half), BF16),
        dma((6,)),
        dma((PIECES,)),
        dma((PIECES * 4,)),
        dma((2,)),
        dma((2,)),
        dma((8,)),
        dma((5 + 2 * DOWN_PIECES,)),
        dma((1 + DOWN_PIECES,)),
        dma((1 + DOWN_PIECES,)),
        dma((1,)),
    ]
    return pl.pallas_call(
        kernel,
        out_shape=jax.ShapeDtypeStruct((rows, half), BF16),
        in_specs=[hbm, vmem, hbm, hbm, vmem, vmem, vmem, vmem, hbm, vmem, hbm, hbm],
        out_specs=hbm,
        scratch_shapes=scratch,
        compiler_params=pltpu.CompilerParams(
            collective_id=0, has_side_effects=True, vmem_limit_bytes=67043328
        ),
    )(
        hidden_in,
        mix_gain[None, :],
        w_value,
        w_gate,
        conv_taps,
        conv_bias[None, :],
        chan_gain[None, :],
        chan_bias[None, :],
        w_back.T,
        feed_gain[None, :],
        w_up,
        w_down,
    )


def solution(mesh):
    placed = (
        P(("rep", "fs"), "tp"),
        P(),
        P("fs", "tp"),
        P("fs", "tp"),
        P(None, "tp"),
        P("tp"),
        P("tp"),
        P("tp"),
        P("tp", "fs"),
        P(),
        P(None, ("fs", "tp")),
        P(("fs", "tp"), None),
    )
    return jax.shard_map(
        shards, mesh=mesh, in_specs=placed, out_specs=P(("rep", "fs"), "tp"), check_vma=False
    )
```

time: 146 us -> 124 us (0.85)
  Pallas kernels: 143 us -> 121 us
    pallas_call x1, Pallas kernels: 143 us -> 121 us  [shards(): pl.pallas_call(kernel, out_shape=jax.ShapeDtypeStruct((rows, half), BF16)...]
where the time goes in v2:
time: 124 us
  Pallas kernels  121 us (98%)
  local copies, waits for them, and re-layouts  2.47 us (2%)
    pallas_call x1, Pallas kernels, shards(): pl.pallas_call(kernel, out_shape=jax.ShapeDtypeStruct((rows, half), BF16)...  121 us

profile of v2, /device:TPU:1, one launch (start us, length us, event | category | flops | bytes accessed | tf_op | source)
XLA Modules:
  0.0 123.9 jit_solution(17222561538878836687)
XLA Ops:
  0.0 121.4 %shard_map.118 = bf16[640,1024]{1,0:T(8,128)(2,1)} custom-call(bf16[640,1024]{1,0:T(8,128)(2,1)} %x_hbm.1, f32[1,2048]{1,0:T(1,128)} %bitcast.7, bf16[64,512]{1,0:T(8,128)(2,1)} %wv_hbm.1, bf16[64,512]{1,0:T(8,128)(2,1)} %wg_hbm.1, f32[31,512]{1,0:T(8,128)} %taps.1, f32[1,512]{1,0:T(1,128)} %bitcast.9, f32[1,512]{1,0:T(1,128)} %bitcast.10, ...), custom_call_target="tpu_custom_call" | custom-call | tf_op jit(solution)/shard_map/pallas_call | solution.py:513
  121.4 2.5 %copy.14 = bf16[640,1024]{1,0:T(8,128)(2,1)} copy(bf16[640,1024]{1,0:T(8,128)(2,1)} %shard_map.118) | data formatting | bytes 2621440

commit v3 on v2

--- a/solution.py
+++ b/solution.py
@@ -13,28 +13,32 @@
 F32 = jnp.float32
 BF16 = jnp.bfloat16
 UP_PIECES = 4
-DOWN_WIDTHS = (256, 256, 128, 128, 128, 128)
-DOWN_FIRST = (0, 256, 512, 640, 768, 896)
+SPLIT = 0
+DOWN_WIDTHS = (256, 256, 256, 128, 128)
+DOWN_FIRST = (0, 256, 512, 768, 896)
 DOWN_PIECES = len(DOWN_WIDTHS)
 PIECES = 2 + UP_PIECES + DOWN_PIECES
-UNITS = (1, 0.5) + (4 / UP_PIECES,) * UP_PIECES + tuple(width / 256 for width in DOWN_WIDTHS)
+UNITS = (1, 0.5) + (4 / UP_PIECES,) * UP_PIECES
+UNITS += tuple(width / 256 / (2 if i == SPLIT else 1) for i, width in enumerate(DOWN_WIDTHS))
 
 ORDER = (
-    "a1", "a0", "a3", "a2", "a7", "a0", "a1", "a10", "a5", "rmsx", "a4", "a6", "a0", "a9", "a3", "a1", "z00", "a4",
-    "a0", "z10", "a5", "a2", "a8", "a6", "a3", "a1", "a11", "z01", "a5", "a2", "a4", "a7", "a0", "z02", "vg0", "a1",
-    "z11", "a9", "a11", "a3", "zw0", "a5", "z12", "vg1", "filter", "a2", "statw", "chan", "a4", "zw1", "a8", "bo",
-    "bw", "a7", "mixw", "second", "a2", "a10", "secw", "a5", "a6", "a4", "rms", "a3", "a8", "upa", "upb", "a7",
-    "hopw", "a6", "forw", "rmsf", "a9", "a8", "a10", "upfa", "a7", "upfb", "a6", "a11", "down0", "a9", "down1", "a8",
-    "a10", "down2", "a11", "a9", "down3", "a10", "down4", "a11", "down5",
+    "a1", "a0", "a6", "a5", "a2", "rmsx", "a9", "a0", "a1", "a6", "a3", "a8", "a4", "a0", "a2", "a1", "a6", "z00",
+    "a9", "a5", "z10", "a0", "z01", "a1", "a3", "a7", "a6", "a5", "a3", "a0", "a1", "a4", "z02", "z11", "vg0", "a2",
+    "a7", "a6", "zw0", "vg1", "z12", "a4", "a3", "y0", "filter", "statw", "y1", "a5", "chan", "zw1", "bo", "bw",
+    "a2", "mixw", "second", "a4", "a8", "a5", "secw", "a10", "a7", "y2", "a3", "rms", "a2", "a4", "upa", "a10", "y3",
+    "a9", "upb", "hopw", "a8", "forw", "a10", "a7", "rmsf", "upfa", "upfb", "a8", "down0", "a9", "a10", "a7",
+    "down1", "a8", "down2", "a10", "a9", "down3", "down4",
 )
 
 
 def kernel(
-    x_hbm, mix_gain, wv_hbm, wg_hbm, taps, conv_bias, chan_gain, chan_bias, wb_hbm, feed_gain, wu_hbm, wd_hbm,
-    out_hbm,
+    x_hbm, mix_gain_hbm, wv_hbm, wg_hbm, taps_hbm, conv_bias_hbm, chan_gain_hbm, chan_bias_hbm, wb_hbm,
+    feed_gain_hbm, wu_hbm, wd_hbm,
+    out_vmem,
     conv_w, up_w, down_w, x_full, normed, padded, filtered, act, stat_own, stat_got,
-    second, hidden, part, part_got, own_sum, ret_send, ret_got, out_vmem,
-    load_sem, send_sem, recv_sem, z_send, z_recv, pair_send, pair_recv, hop_send, hop_recv, out_sem,
+    mix_gain, taps, conv_bias, chan_gain, chan_bias, feed_gain,
+    second, hidden, part, part_got, own_sum, ret_send, ret_got,
+    relay, load_sem, send_sem, recv_sem, z_send, z_recv, pair_send, pair_recv, hop_send, hop_recv, y_send, y_recv,
 ):
     rows, half = x_hbm.shape
     features = 2 * half
@@ -87,10 +91,17 @@
     for index in range(DOWN_PIECES):
         width, first = DOWN_WIDTHS[index], DOWN_FIRST[index]
         for h in range(2):
-            src = wd_hbm.at[:, pl.ds(h * half + first, width)]
-            dst = down_w.at[y, of(0, x, block), pl.ds(2 * first + h * width, width)]
-            loads.append(pltpu.make_async_copy(src, dst, load_sem.at[5]))
-    for load in loads:
+            size, shift, sem = width, 0, 5
+            if index == SPLIT:
+                size, sem = width // 2, 12
+                shift = z_hi * size
+            src = wd_hbm.at[:, pl.ds(pl.multiple_of(h * half + first + shift, 128), size)]
+            dst = down_w.at[y, of(0, x, block), pl.ds(pl.multiple_of(2 * first + h * width + shift, 128), size)]
+            loads.append(pltpu.make_async_copy(src, dst, load_sem.at[sem]))
+    small = [(mix_gain_hbm, mix_gain), (taps_hbm, taps), (conv_bias_hbm, conv_bias)]
+    small += [(chan_gain_hbm, chan_gain), (chan_bias_hbm, chan_bias), (feed_gain_hbm, feed_gain)]
+    small_loads = [pltpu.make_async_copy(src, dst, load_sem.at[6 + i]) for i, (src, dst) in enumerate(small)]
+    for load in loads + small_loads:
         load.start()
 
     barrier = pltpu.get_barrier_semaphore()
@@ -126,11 +137,35 @@
 
         return view
 
+    def split_cols(colour, which):
+        width, first = DOWN_WIDTHS[SPLIT], DOWN_FIRST[SPLIT]
+        return pl.ds(pl.multiple_of(2 * first + colour * width + which * (width // 2), 128), width // 2)
+
+    def split_send(part):
+        rows_of = pl.ds(part * 2, 2)
+        for colour, device in ((0, at_z(z_next)), (1, at_z(z_prev))):
+            src = down_w.at[rows_of, :, split_cols(colour, z_hi)]
+            remote(src, relay.at[colour, rows_of], y_send.at[part], y_recv.at[part], device).start()
+
+    def split_wait(number):
+        both = relay.at[:, 0:2]
+        pltpu.make_async_copy(both, both, y_recv.at[number]).wait()
+        pltpu.make_async_copy(both, both, y_send.at[number]).wait()
+
+    def split_pass(part):
+        split_wait(part)
+        rows_of = pl.ds(part * 2, 2)
+        for colour, device, source in ((0, at_z(z_next), z_prev), (1, at_z(z_prev), z_next)):
+            dst = down_w.at[rows_of, :, split_cols(colour, source // 2)]
+            remote(relay.at[colour, rows_of], dst, y_send.at[2 + part], y_recv.at[2 + part], device).start()
+
     def down_piece(index):
         width, first = DOWN_WIDTHS[index], DOWN_FIRST[index]
 
         def view(what, yy, xx, colour, part):
             cols = pl.ds(2 * first + colour * width, width)
+            if index == SPLIT:
+                cols = split_cols(colour, z_hi)
             size = block if part is None else block // 2
             rows_of_block = pl.ds(pl.multiple_of(xx * block + (part or 0) * size, size), size)
             if what == "block":
@@ -226,8 +261,8 @@
         scale = gain[...]
 
         def body(i, carry):
-            at = pl.ds(pl.multiple_of(first + i * step_rows, step_rows), step_rows)
-            values = src[at, :].astype(F32)
+            at = pl.ds(pl.multiple_of(i * step_rows, step_rows), step_rows)
+            values = src[pl.ds(pl.multiple_of(first + i * step_rows, step_rows), step_rows), :].astype(F32)
             mean = jnp.sum(values * values, axis=1, keepdims=True) * (1.0 / features)
             dst[at, :] = (values * lax.rsqrt(mean + 1e-6) * scale).astype(BF16)
             return carry
@@ -251,6 +286,8 @@
 
     def first_norm():
         loads[4].wait()
+        for load in small_loads:
+            load.wait()
         x_swap.wait()
         rms(x_full, normed, mix_gain, 0, rows)
         padded[:, 0:32, :] = jnp.zeros((sequences, 32, channels), F32)
@@ -260,7 +297,7 @@
     def plane_dot(which, cols):
         at = pl.ds(pl.multiple_of(which * half, half), half)
         weights = conv_w[pl.ds(which * SIDE, SIDE), :, cols].reshape(half, tile)
-        return jnp.dot(normed[0:rows, at], weights, preferred_element_type=F32)
+        return jnp.dot(normed[:, at], weights, preferred_element_type=F32)
 
     def value_gate_own():
         for n in range(2 * channels // tile):
@@ -335,11 +372,11 @@
             hop.start()
         second_swap.start()
 
-    def up(first, begin, end):
+    def up(source, first, begin, end):
         at = pl.ds(first, rows)
 
         def body(i, carry):
-            product = jnp.dot(normed[at, :], up_w[i], preferred_element_type=F32)
+            product = jnp.dot(source[...], up_w[i], preferred_element_type=F32)
             positive = jnp.maximum(product, 0.0)
             hidden[at, pl.ds(pl.multiple_of(i * SIDE * block, SIDE * block), SIDE * block)] = (positive * positive).astype(BF16)
             return carry
@@ -401,10 +438,11 @@
         pltpu.make_async_copy(both, both, hop_recv.at[1 + index]).wait()
         pltpu.make_async_copy(both, both, hop_send.at[1 + index]).wait()
         out_vmem[:, cols] = (own_sum[:, cols] + ret_got[:, cols].astype(F32)).astype(BF16)
-        copy = pltpu.make_async_copy(out_vmem.at[:, cols], out_hbm.at[:, cols], out_sem.at[0])
-        copy.start()
 
     def down_step(index):
+        if index == SPLIT:
+            split_wait(2)
+            split_wait(3)
         down(index)
         send_back(index)
         if index:
@@ -427,22 +465,24 @@
         second=residual,
         secw=second_swap.wait,
         rms=lambda: rms(second, normed, feed_gain, 0, rows),
-        upa=lambda: up(0, 0, SIDE // 2),
-        upb=lambda: up(0, SIDE // 2, SIDE),
+        upa=lambda: up(normed, 0, 0, SIDE // 2),
+        upb=lambda: up(normed, 0, SIDE // 2, SIDE),
         hopw=arrived,
         forw=foreign_swap.wait,
-        rmsf=lambda: rms(second, normed, feed_gain, rows, rows),
-        upfa=lambda: up(rows, 0, SIDE // 2),
-        upfb=lambda: up(rows, SIDE // 2, SIDE),
+        rmsf=lambda: rms(second, x_full, feed_gain, rows, rows),
+        upfa=lambda: up(x_full, rows, 0, SIDE // 2),
+        upfb=lambda: up(x_full, rows, SIDE // 2, SIDE),
     )
     for index in range(DOWN_PIECES):
         actions[f"down{index}"] = functools.partial(down_step, index)
 
     first_load = {0: (0, 1), 1: (2,)}
     first_load.update({piece: (3,) for piece in ups})
-    first_load.update({piece: (5,) for piece in downs})
-    whole_down = down_w.at[y, of(0, x, block), :]
-    loads[5:] = [pltpu.make_async_copy(whole_down, whole_down, load_sem.at[5])]
+    first_load.update({piece: (6 if i == SPLIT else 5,) for i, piece in enumerate(downs)})
+    split_width = DOWN_WIDTHS[SPLIT]
+    most = down_w.at[y, of(0, x, block), 0 : features - 2 * split_width]
+    few = down_w.at[y, of(0, x, block), 0:split_width]
+    loads[5:] = [pltpu.make_async_copy(most, most, load_sem.at[5]), pltpu.make_async_copy(few, few, load_sem.at[12])]
     loaded = set()
 
     x_swap.start()
@@ -454,6 +494,10 @@
                     loads[number].wait()
                     loaded.add(number)
             advance(piece)
+        elif name[0] == "y":
+            number = int(name[1:])
+            with jax.named_scope(name):
+                (split_send if number < 2 else split_pass)(number % 2)
         elif name[0] == "z" and name[1:].isdigit():
             z_go(int(name[1]), int(name[2]))
         else:
@@ -464,7 +508,6 @@
     finish(DOWN_PIECES - 2)
     with jax.named_scope("last"):
         finish(DOWN_PIECES - 1)
-        pltpu.make_async_copy(out_vmem, out_hbm, out_sem.at[0]).wait()
     assert all(counts[piece] == 5 for piece in range(PIECES)), counts
 
 
@@ -485,12 +528,18 @@
         pltpu.VMEM((SIDE, features, SIDE * block), BF16),
         pltpu.VMEM((SIDE, SIDE * block, features), BF16),
         pltpu.VMEM((rows, features), BF16),
-        pltpu.VMEM((2 * rows, features), BF16),
+        pltpu.VMEM((rows, features), BF16),
         pltpu.VMEM((sequences, 32 + LEN, channels), F32),
         pltpu.VMEM((rows, channels), F32),
         pltpu.VMEM((rows, channels), BF16),
         pltpu.VMEM((2, rows, 128), F32),
         pltpu.VMEM((2, rows, 128), F32),
+        pltpu.VMEM((1, features), F32),
+        pltpu.VMEM(conv_taps.shape, F32),
+        pltpu.VMEM((1, channels), F32),
+        pltpu.VMEM((1, channels), F32),
+        pltpu.VMEM((1, channels), F32),
+        pltpu.VMEM((1, features), F32),
         pltpu.VMEM((2 * rows, features), BF16),
         pltpu.VMEM((2 * rows, plane * block), BF16),
         pltpu.VMEM((2, 2 * rows, half), BF16),
@@ -498,8 +547,8 @@
         pltpu.VMEM((rows, half), F32),
         pltpu.VMEM((rows, half), BF16),
         pltpu.VMEM((rows, half), BF16),
-        pltpu.VMEM((rows, half), BF16),
-        dma((6,)),
+        pltpu.VMEM((2, SIDE, SIDE * block, DOWN_WIDTHS[SPLIT] // 2), BF16),
+        dma((13,)),
         dma((PIECES,)),
         dma((PIECES * 4,)),
         dma((2,)),
@@ -508,16 +557,17 @@
         dma((5 + 2 * DOWN_PIECES,)),
         dma((1 + DOWN_PIECES,)),
         dma((1 + DOWN_PIECES,)),
-        dma((1,)),
+        dma((4,)),
+        dma((4,)),
     ]
     return pl.pallas_call(
         kernel,
-        out_shape=jax.ShapeDtypeStruct((rows, half), BF16),
-        in_specs=[hbm, vmem, hbm, hbm, vmem, vmem, vmem, vmem, hbm, vmem, hbm, hbm],
-        out_specs=hbm,
+        out_shape=pltpu.VMEM((rows, half), BF16),
+        in_specs=[hbm] * 12,
+        out_specs=vmem,
         scratch_shapes=scratch,
         compiler_params=pltpu.CompilerParams(
-            collective_id=0, has_side_effects=True, vmem_limit_bytes=67043328
+            collective_id=0, has_side_effects=True, vmem_limit_bytes=61 * 2**20
         ),
     )(
         hidden_in,

time: 124 us -> 119 us (0.960)
  Pallas kernels: 121 us -> 118 us
  local copies, waits for them, and re-layouts: 2.47 us -> 1.06 us
    pallas_call x1, Pallas kernels: 121 us -> 118 us  [shards(): pl.pallas_call(kernel, out_shape=pltpu.VMEM((rows, half), BF16), in_specs...]
    unnamed x1, local copies, waits for them, and re-layouts: 2.47 us -> 1.06 us
where the time goes in v3:
time: 119 us
  Pallas kernels  118 us (99%)
    pallas_call x1, Pallas kernels, shards(): pl.pallas_call(kernel, out_shape=pltpu.VMEM((rows, half), BF16), in_specs...  118 us

profile of v3, /device:TPU:1, one launch (start us, length us, event | category | flops | bytes accessed | tf_op | source)
XLA Modules:
  0.0 118.7 jit_solution(7833808132458041116)
XLA Ops:
  0.0 117.7 %shard_map.118 = bf16[640,1024]{1,0:T(8,128)(2,1)S(1)} custom-call(bf16[640,1024]{1,0:T(8,128)(2,1)} %x_hbm.1, f32[1,2048]{1,0:T(1,128)} %bitcast.7, bf16[64,512]{1,0:T(8,128)(2,1)} %wv_hbm.1, bf16[64,512]{1,0:T(8,128)(2,1)} %wg_hbm.1, f32[31,512]{1,0:T(8,128)} %taps_hbm.1, f32[1,512]{1,0:T(1,128)} %bitcast.9, f32[1,512]{1,0:T(1,128)} %bitcast.10, ...), custom_call_target="tpu_custom_call" | custom-call | tf_op jit(solution)/shard_map/pallas_call | solution.py:563
  117.7 1.1 copy.14

commit v4 on v3

--- a/solution.py
+++ b/solution.py
@@ -22,12 +22,13 @@
 UNITS += tuple(width / 256 / (2 if i == SPLIT else 1) for i, width in enumerate(DOWN_WIDTHS))
 
 ORDER = (
-    "a1", "a0", "a6", "a5", "a2", "rmsx", "a9", "a0", "a1", "a6", "a3", "a8", "a4", "a0", "a2", "a1", "a6", "z00",
-    "a9", "a5", "z10", "a0", "z01", "a1", "a3", "a7", "a6", "a5", "a3", "a0", "a1", "a4", "z02", "z11", "vg0", "a2",
-    "a7", "a6", "zw0", "vg1", "z12", "a4", "a3", "y0", "filter", "statw", "y1", "a5", "chan", "zw1", "bo", "bw",
-    "a2", "mixw", "second", "a4", "a8", "a5", "secw", "a10", "a7", "y2", "a3", "rms", "a2", "a4", "upa", "a10", "y3",
-    "a9", "upb", "hopw", "a8", "forw", "a10", "a7", "rmsf", "upfa", "upfb", "a8", "down0", "a9", "a10", "a7",
-    "down1", "a8", "down2", "a10", "a9", "down3", "down4",
+    "a0", "a5", "a1", "a6", "a8", "a0", "a10", "a3", "a1", "a7", "a5", "a0", "rmsx", "a3", "a1", "a6", "z10", "z00",
+    "a9", "a0", "z01", "a4", "a6", "a10", "a1", "a2", "a3", "a0", "z02", "a6", "vg0", "z11", "a1", "a2", "a4", "a5",
+    "a7", "z12", "a6", "a3", "zw0", "vg1", "a4", "y0", "filter", "y1", "a2", "statw", "chan", "a5", "zw1", "bo",
+    "a8", "bw", "mixw", "second", "a4", "a2", "secw", "y2", "rms0", "a7", "a5", "a3", "rms1", "hopw0", "a8", "a4",
+    "a9", "a2", "forw0", "rmsf0", "upf00", "upf01", "hopw1", "y3", "a7", "up0", "up1", "forw1", "a10", "rmsf1",
+    "upf10", "a9", "upf11", "a8", "dF0", "up2", "sb0", "a7", "up3", "dF1", "a9", "a10", "dO0", "sb1", "a8", "dF2",
+    "dO1", "sb2", "a9", "dF3", "dO2", "sb3", "a10", "dF4", "dO3", "sb4", "dO4",
 )
 
 
@@ -257,11 +258,11 @@
     ups = list(range(2, 2 + UP_PIECES))
     downs = list(range(2 + UP_PIECES, PIECES))
 
-    def rms(src, dst, gain, first, count, step_rows=32):
+    def rms(src, dst, gain, first, count, step_rows=32, to=0):
         scale = gain[...]
 
         def body(i, carry):
-            at = pl.ds(pl.multiple_of(i * step_rows, step_rows), step_rows)
+            at = pl.ds(pl.multiple_of(to + i * step_rows, step_rows), step_rows)
             values = src[pl.ds(pl.multiple_of(first + i * step_rows, step_rows), step_rows), :].astype(F32)
             mean = jnp.sum(values * values, axis=1, keepdims=True) * (1.0 / features)
             dst[at, :] = (values * lax.rsqrt(mean + 1e-6) * scale).astype(BF16)
@@ -271,17 +272,28 @@
 
     mine = of(0, core, half)
     own, foreign = pl.ds(0, rows), pl.ds(rows, rows)
-    low, high = pl.ds(0, part_rows), pl.ds(part_rows, part_rows)
-    from_prev, from_next = pl.ds(rows, part_rows), pl.ds(rows + part_rows, part_rows)
     mix_send, mix_got = part.at[0, 0:rows, :], part_got.at[0:rows, :]
     x_swap = remote(x_hbm, x_full.at[:, mine], pair_send.at[0], pair_recv.at[0], partner)
     stat_swap = remote(stat_own, stat_got, pair_send.at[1], pair_recv.at[1], partner)
     mix_swap = remote(mix_send, mix_got, pair_send.at[2], pair_recv.at[2], partner)
     second_swap = remote(second.at[own, mine], second.at[own, mine], pair_send.at[3], pair_recv.at[3], partner)
-    foreign_swap = remote(second.at[foreign, mine], second.at[foreign, mine], pair_send.at[4], pair_recv.at[4], partner)
+    part_rows, strip = rows // 2, rows // 4
+
+    def strip_of(first, k, way):
+        return pl.ds(first + k * part_rows + way * strip, strip)
+
+    def home_of(k, way):
+        return pl.ds(way * part_rows + k * strip, strip)
+
+    far = [second.at[pl.ds(rows + k * part_rows, part_rows), mine] for k in range(2)]
+    foreign_swap = [remote(far[k], far[k], pair_send.at[4 + k], pair_recv.at[4 + k], partner) for k in range(2)]
     hops = [
-        remote(second.at[low, mine], second.at[from_prev, mine], hop_send.at[0], hop_recv.at[0], at_z(z_next)),
-        remote(second.at[high, mine], second.at[from_next, mine], hop_send.at[0], hop_recv.at[0], at_z(z_prev)),
+        remote(
+            second.at[home_of(k, way), mine], second.at[strip_of(rows, k, way), mine],
+            hop_send.at[k], hop_recv.at[k], at_z((z_next, z_prev)[way]),
+        )
+        for k in range(2)
+        for way in range(2)
     ]
 
     def first_norm():
@@ -373,7 +385,7 @@
         second_swap.start()
 
     def up(source, first, begin, end):
-        at = pl.ds(first, rows)
+        at = pl.ds(first, source.shape[0])
 
         def body(i, carry):
             product = jnp.dot(source[...], up_w[i], preferred_element_type=F32)
@@ -383,72 +395,63 @@
 
         lax.fori_loop(begin, end, body, 0)
 
-    def arrived():
-        both = second.at[foreign, mine]
-        pltpu.make_async_copy(both, both, hop_recv.at[0]).wait()
-        pltpu.make_async_copy(both, both, hop_send.at[0]).wait()
-        foreign_swap.start()
+    def arrived(k):
+        pltpu.make_async_copy(far[k], far[k], hop_recv.at[k]).wait()
+        pltpu.make_async_copy(far[k], far[k], hop_send.at[k]).wait()
+        foreign_swap[k].start()
+
+    def far_norm(k):
+        rms(second, x_full, feed_gain, rows + k * part_rows, part_rows, to=k * part_rows)
+
+    def far_up(k, begin):
+        up(x_full.at[pl.ds(k * part_rows, part_rows), :], rows + k * part_rows, begin, begin + SIDE // 2)
 
     swaps = {}
 
-    def down(index):
+    def down(index, number):
         width, first = DOWN_WIDTHS[index], DOWN_FIRST[index]
         cols = pl.ds(first, width)
         depth = SIDE * SIDE * block
-        swaps[index] = []
-        for number, at in enumerate((foreign, own)):
-
-            def body(i, carry):
-                chunk = pl.ds(pl.multiple_of(at.start + i * part_rows, part_rows), part_rows)
-                weights = down_w[:, :, pl.ds(2 * first, 2 * width)].reshape(depth, 2 * width)
-                product = jnp.dot(hidden[chunk, :], weights, preferred_element_type=F32).astype(BF16)
-                part[0, chunk, cols] = product[:, :width]
-                part[1, chunk, cols] = product[:, width:]
-                return carry
-
-            lax.fori_loop(0, 2, body, 0)
-            slot = 5 + 2 * index + number
-            swap = remote(part.at[other, at, cols], part_got.at[at, cols], pair_send.at[5 if number == 0 else 6 + index % 2], pair_recv.at[slot], partner)
-            swap.start()
-            swaps[index].append(swap)
+        at = (foreign, own)[number]
+        many = 1 if width >= 256 else 2
+        if index == SPLIT and number == 0:
+            split_wait(2)
+            split_wait(3)
+
+        def body(i, carry):
+            chunk = pl.ds(pl.multiple_of(at.start + i * (rows // many), rows // many), rows // many)
+            weights = down_w[:, :, pl.ds(2 * first, 2 * width)].reshape(depth, 2 * width)
+            product = jnp.dot(hidden[chunk, :], weights, preferred_element_type=F32).astype(BF16)
+            part[0, chunk, cols] = product[:, :width]
+            part[1, chunk, cols] = product[:, width:]
+            return carry
+
+        lax.fori_loop(0, many, body, 0)
+        sem = pair_send.at[6 + number * (1 + index)]
+        swap = remote(part.at[other, at, cols], part_got.at[at, cols], sem, pair_recv.at[6 + 2 * index + number], partner)
+        swap.start()
+        swaps[index, number] = swap
 
     def send_back(index):
         width, first = DOWN_WIDTHS[index], DOWN_FIRST[index]
         cols = pl.ds(first, width)
-        swaps[index][0].wait()
+        swaps[index, 0].wait()
         ret_send[:, cols] = (part[core, foreign, cols].astype(F32) + part_got[foreign, cols].astype(F32)).astype(BF16)
-        for at, device in ((low, at_z(z_prev)), (high, at_z(z_next))):
-            slot = 1 + index
-            back = remote(ret_send.at[at, cols], ret_got.at[at, cols], hop_send.at[slot], hop_recv.at[slot], device)
-            back.start()
-
-    def sum_own(index):
-        width, first = DOWN_WIDTHS[index], DOWN_FIRST[index]
-        cols = pl.ds(first, width)
-        swaps[index][1].wait()
-        there = pl.ds(pl.multiple_of(core * half + first, 128), width)
-        own_sum[:, cols] = (
-            second[own, there].astype(F32) + part[core, own, cols].astype(F32) + part_got[own, cols].astype(F32)
-        )
+        for k in range(2):
+            for way, device in ((0, at_z(z_prev)), (1, at_z(z_next))):
+                src, dst = ret_send.at[strip_of(0, k, way), cols], ret_got.at[home_of(k, way), cols]
+                remote(src, dst, hop_send.at[2 + index], hop_recv.at[2 + index], device).start()
 
     def finish(index):
         width, first = DOWN_WIDTHS[index], DOWN_FIRST[index]
         cols = pl.ds(first, width)
+        swaps[index, 1].wait()
         both = ret_got.at[:, cols]
-        pltpu.make_async_copy(both, both, hop_recv.at[1 + index]).wait()
-        pltpu.make_async_copy(both, both, hop_send.at[1 + index]).wait()
-        out_vmem[:, cols] = (own_sum[:, cols] + ret_got[:, cols].astype(F32)).astype(BF16)
-
-    def down_step(index):
-        if index == SPLIT:
-            split_wait(2)
-            split_wait(3)
-        down(index)
-        send_back(index)
-        if index:
-            sum_own(index - 1)
-        if index > 1:
-            finish(index - 2)
+        pltpu.make_async_copy(both, both, hop_recv.at[2 + index]).wait()
+        pltpu.make_async_copy(both, both, hop_send.at[2 + index]).wait()
+        there = pl.ds(pl.multiple_of(core * half + first, 128), width)
+        total = second[own, there].astype(F32) + part[core, own, cols].astype(F32) + part_got[own, cols].astype(F32)
+        out_vmem[:, cols] = (total + ret_got[:, cols].astype(F32)).astype(BF16)
 
     actions = dict(
         rmsx=first_norm,
@@ -464,17 +467,24 @@
         mixw=mix_swap.wait,
         second=residual,
         secw=second_swap.wait,
-        rms=lambda: rms(second, normed, feed_gain, 0, rows),
-        upa=lambda: up(normed, 0, 0, SIDE // 2),
-        upb=lambda: up(normed, 0, SIDE // 2, SIDE),
-        hopw=arrived,
-        forw=foreign_swap.wait,
-        rmsf=lambda: rms(second, x_full, feed_gain, rows, rows),
-        upfa=lambda: up(x_full, rows, 0, SIDE // 2),
-        upfb=lambda: up(x_full, rows, SIDE // 2, SIDE),
+        rms0=lambda: rms(second, normed, feed_gain, 0, part_rows),
+        rms1=lambda: rms(second, normed, feed_gain, part_rows, part_rows, to=part_rows),
+        hopw0=lambda: arrived(0),
+        hopw1=lambda: arrived(1),
+        forw0=foreign_swap[0].wait,
+        forw1=foreign_swap[1].wait,
+        rmsf0=lambda: far_norm(0),
+        rmsf1=lambda: far_norm(1),
     )
+    for index in range(SIDE):
+        actions[f"up{index}"] = functools.partial(up, normed, 0, index, index + 1)
+    for k in range(2):
+        for index in range(2):
+            actions[f"upf{k}{index}"] = functools.partial(far_up, k, 2 * index)
     for index in range(DOWN_PIECES):
-        actions[f"down{index}"] = functools.partial(down_step, index)
+        actions[f"dF{index}"] = functools.partial(down, index, 0)
+        actions[f"dO{index}"] = functools.partial(down, index, 1)
+        actions[f"sb{index}"] = functools.partial(send_back, index)
 
     first_load = {0: (0, 1), 1: (2,)}
     first_load.update({piece: (3,) for piece in ups})
@@ -504,10 +514,9 @@
             with jax.named_scope(name):
                 actions[name]()
 
-    sum_own(DOWN_PIECES - 1)
-    finish(DOWN_PIECES - 2)
-    with jax.named_scope("last"):
-        finish(DOWN_PIECES - 1)
+    for index in range(DOWN_PIECES):
+        with jax.named_scope(f"finish{index}"):
+            finish(index)
     assert all(counts[piece] == 5 for piece in range(PIECES)), counts
 
 
@@ -553,10 +562,10 @@
         dma((PIECES * 4,)),
         dma((2,)),
         dma((2,)),
-        dma((8,)),
-        dma((5 + 2 * DOWN_PIECES,)),
-        dma((1 + DOWN_PIECES,)),
-        dma((1 + DOWN_PIECES,)),
+        dma((7 + DOWN_PIECES,)),
+        dma((6 + 2 * DOWN_PIECES,)),
+        dma((2 + DOWN_PIECES,)),
+        dma((2 + DOWN_PIECES,)),
         dma((4,)),
         dma((4,)),
     ]

time: 119 us -> 117 us (0.983)
  Pallas kernels: 118 us -> 116 us
    pallas_call x1, Pallas kernels: 118 us -> 116 us  [shards(): pl.pallas_call(kernel, out_shape=pltpu.VMEM((rows, half), BF16), in_specs...]
where the time goes in v4:
time: 117 us
  Pallas kernels  116 us (99%)
    pallas_call x1, Pallas kernels, shards(): pl.pallas_call(kernel, out_shape=pltpu.VMEM((rows, half), BF16), in_specs...  116 us

profile of v4, /device:TPU:1, one launch (start us, length us, event | category | flops | bytes accessed | tf_op | source)
XLA Modules:
  0.0 116.9 jit_solution(14876080135600211923)
XLA Ops:
  0.0 115.8 %shard_map.118 = bf16[640,1024]{1,0:T(8,128)(2,1)S(1)} custom-call(bf16[640,1024]{1,0:T(8,128)(2,1)} %x_hbm.1, f32[1,2048]{1,0:T(1,128)} %bitcast.7, bf16[64,512]{1,0:T(8,128)(2,1)} %wv_hbm.1, bf16[64,512]{1,0:T(8,128)(2,1)} %wg_hbm.1, f32[31,512]{1,0:T(8,128)} %taps_hbm.1, f32[1,512]{1,0:T(1,128)} %bitcast.9, f32[1,512]{1,0:T(1,128)} %bitcast.10, ...), custom_call_target="tpu_custom_call" | custom-call | tf_op jit(solution)/shard_map/pallas_call | solution.py:572
  115.8 1.1 copy.14

commit v5 on v4

--- a/solution.py
+++ b/solution.py
@@ -268,7 +268,7 @@
             dst[at, :] = (values * lax.rsqrt(mean + 1e-6) * scale).astype(BF16)
             return carry
 
-        lax.fori_loop(0, count // step_rows, body, 0)
+        lax.fori_loop(0, count // step_rows, body, 0, unroll=2)
 
     mine = of(0, core, half)
     own, foreign = pl.ds(0, rows), pl.ds(rows, rows)

time: 117 us -> 117 us (level)
  no operation moved by 1% of the time
where the time goes in v5:
time: 117 us
  Pallas kernels  116 us (99%)
    pallas_call x1, Pallas kernels, shards(): pl.pallas_call(kernel, out_shape=pltpu.VMEM((rows, half), BF16), in_specs...  116 us

profile of v5, /device:TPU:1, one launch (start us, length us, event | category | flops | bytes accessed | tf_op | source)
XLA Modules:
  0.0 116.9 jit_solution(103013862348570203)
XLA Ops:
  0.0 115.8 %shard_map.118 = bf16[640,1024]{1,0:T(8,128)(2,1)S(1)} custom-call(bf16[640,1024]{1,0:T(8,128)(2,1)} %x_hbm.1, f32[1,2048]{1,0:T(1,128)} %bitcast.7, bf16[64,512]{1,0:T(8,128)(2,1)} %wv_hbm.1, bf16[64,512]{1,0:T(8,128)(2,1)} %wg_hbm.1, f32[31,512]{1,0:T(8,128)} %taps_hbm.1, f32[1,512]{1,0:T(1,128)} %bitcast.9, f32[1,512]{1,0:T(1,128)} %bitcast.10, ...), custom_call_target="tpu_custom_call" | custom-call | tf_op jit(solution)/shard_map/pallas_call | solution.py:572
  115.8 1.1 copy.14
